TPU v7x, 256 devices: a whole 4x4x8 slice. The times are simulated.
256 devices in a mesh: ep: 16 (over y, x), tp: 16 (over z, core).
Axes of the slice: x: 4, y: 4, z: 8, core: 2. Of those that a mesh axis runs over, the one named last changes fastest.
Arguments:
- mix_tokens: bfloat16 [4096, 4096], P('ep'), may hold values from -6 to 6
- mix_gain: float32 [4096], replicated, may hold values from 0.1 to 1.9
- value_weight: bfloat16 [4096, 2048], P(None, 'tp'), may hold values from -0.09375 to 0.09375
- inner_weight: bfloat16 [4096, 2048], P(None, 'tp'), may hold values from -0.09375 to 0.09375
- outer_weight: bfloat16 [4096, 2048], P(None, 'tp'), may hold values from -0.09375 to 0.09375
- conv_taps: float32 [3, 2048], P(None, 'tp'), may hold values from -3 to 3
- mix_weight: bfloat16 [2048, 4096], P('tp'), may hold values from -0.125 to 0.125
- moe_tokens: bfloat16 [4096, 4096], P('ep'), may hold values from -6 to 6
- moe_gain: float32 [4096], replicated, may hold values from 0.1 to 1.9
- router_group: bfloat16 [4096, 4], replicated, may hold values from -0.09375 to 0.09375
- router_expert: bfloat16 [4096, 16], replicated, may hold values from -0.09375 to 0.09375
- expert_routes: int32 [4096, 2], P('ep'), may hold values from 0 to 15, as said below
- gate_weight: bfloat16 [16, 4096, 2048], P('ep', None, 'tp'), may hold values from -0.09375 to 0.09375
- up_weight: bfloat16 [16, 4096, 2048], P('ep', None, 'tp'), may hold values from -0.09375 to 0.09375
- down_weight: bfloat16 [16, 2048, 4096], P('ep', 'tp'), may hold values from -0.5 to 0.5
Outputs:
- mixer_out: bfloat16 [4096, 4096], P(('ep', 'tp'))
- expert_out: bfloat16 [4096, 4096], P(('ep', 'tp'))
Inputs may be any that keep to these rules, and one draw needn't show every extreme that they name: `expert_routes`: the two experts of a row are different and lie in one group of 4 consecutive expert numbers. In each aligned block of 16 rows no expert is named more than 4 times, and in every draw some experts are named exactly 4 times in every block.
All inputs are finite; a program needn't handle non-finite values.
Results may differ from a plain program's by a relative error of at most 0.0076.
Values may be sent and summed in bfloat16 or wider, within the bound.
No kernel may reach another device: no remote copies, remote signals or barrier semaphores. Data moves between devices by JAX's collectives and lax.ppermute only.
A program may use at most 128 MiB of HBM per device.

v0:
```python
import jax
import jax.numpy as jnp
from jax import lax
from jax.sharding import PartitionSpec as P

TAPS = 3
EXPERTS = 16
GROUPS = 4
TOPK = 2
MOE_SHARE = 16
EPG = 4
CAP = 4


def from_behind(value, axis, steps):
    count = lax.axis_size(axis)
    initial, last = (max(0, -steps), min(count, count - steps))
    return lax.ppermute(value, axis, [(source, source + steps) for source in range(initial, last)])


def rms_rows(inputs, gain_vec):
    values = inputs.astype(jnp.float32)
    inverse = lax.rsqrt(jnp.mean(values * values, axis=-1, keepdims=True) + 1e-06)
    return (values * inverse * gain_vec).astype(jnp.bfloat16)


def route_weights(normed, routes, router_group, router_expert):
    group_logit = jnp.dot(normed, router_group, preferred_element_type=jnp.float32)
    expert_logit = jnp.dot(normed, router_expert, preferred_element_type=jnp.float32)
    group_exp = jnp.exp(group_logit)
    group_id = routes[:, 0] // EPG
    group_pick = (group_id[:, None] == jnp.arange(GROUPS, dtype=jnp.int32)[None, :]).astype(
        jnp.float32
    )
    group_gate = jnp.sum(group_exp * group_pick, axis=1) / jnp.sum(group_exp, axis=1)
    expert_pick = (
        routes[:, :, None] == jnp.arange(EXPERTS, dtype=jnp.int32)[None, None, :]
    ).astype(jnp.float32)
    chosen = jnp.exp(jnp.sum(expert_logit[:, None, :] * expert_pick, axis=2))
    return group_gate[:, None] * chosen / jnp.sum(chosen, axis=1, keepdims=True)


def block_ranks(routes):
    blocks = routes.shape[0]
    entries = routes.reshape(blocks, MOE_SHARE * TOPK)
    one_hot = (entries[:, :, None] == jnp.arange(EXPERTS, dtype=jnp.int32)[None, None, :]).astype(
        jnp.int32
    )
    before = jnp.cumsum(one_hot, axis=1) - one_hot
    return jnp.sum(before * one_hot, axis=2).reshape(routes.shape)


def dispatch_rows(normed, routes):
    slot_ids = routes * CAP + block_ranks(routes)
    targets = jnp.arange(EXPERTS * CAP, dtype=jnp.int32)
    select = (slot_ids[:, None, :, :] == targets[None, :, None, None]).astype(jnp.int32)
    select = jnp.sum(select, axis=3).astype(jnp.bfloat16)
    placed = jnp.einsum("bcs,bsd->bcd", select, normed, preferred_element_type=jnp.float32)
    return placed.astype(jnp.bfloat16).reshape(normed.shape[0], EXPERTS, CAP, normed.shape[2])


def expert_hidden(arrived, gate_weight, up_weight):
    gate_proj = jnp.einsum(
        "besd,edf->besf", arrived, gate_weight, preferred_element_type=jnp.float32
    )
    up_proj = jnp.einsum("besd,edf->besf", arrived, up_weight, preferred_element_type=jnp.float32)
    return (jax.nn.silu(gate_proj) * up_proj).astype(jnp.bfloat16)


def mixer_half(
    mix_tokens, mix_gain, value_weight, inner_weight, outer_weight, conv_taps, mix_weight
):
    normed = rms_rows(mix_tokens, mix_gain)
    value_proj = jnp.dot(normed, value_weight, preferred_element_type=jnp.float32)
    inner_proj = jnp.dot(normed, inner_weight, preferred_element_type=jnp.float32)
    outer_proj = jnp.dot(normed, outer_weight, preferred_element_type=jnp.float32)
    gated_in = (inner_proj * value_proj).astype(jnp.bfloat16)
    earlier = from_behind(gated_in[gated_in.shape[0] - (TAPS - 1) :], "ep", 1)
    padded = jnp.concatenate([earlier, gated_in], axis=0).astype(jnp.float32)
    seq_rows = gated_in.shape[0]
    mixed_conv = conv_taps[0] * padded[0:seq_rows]
    for tap_index in range(1, TAPS):
        mixed_conv = mixed_conv + conv_taps[tap_index] * padded[tap_index : tap_index + seq_rows]
    conv_out = (outer_proj * mixed_conv).astype(jnp.bfloat16)
    summed = lax.psum_scatter(
        jnp.dot(conv_out, mix_weight, preferred_element_type=jnp.float32),
        "tp",
        scatter_dimension=0,
        tiled=True,
    )
    return summed.astype(jnp.bfloat16)


def local(
    mix_tokens,
    mix_gain,
    value_weight,
    inner_weight,
    outer_weight,
    conv_taps,
    mix_weight,
    moe_tokens,
    moe_gain,
    router_group,
    router_expert,
    expert_routes,
    gate_weight,
    up_weight,
    down_weight,
):
    mixer_out = mixer_half(
        mix_tokens, mix_gain, value_weight, inner_weight, outer_weight, conv_taps, mix_weight
    )
    tp_index = lax.axis_index("tp")
    model_width = moe_tokens.shape[1]
    own_routes = lax.dynamic_slice_in_dim(expert_routes, tp_index * MOE_SHARE, MOE_SHARE, 0)
    own_tokens = lax.dynamic_slice_in_dim(moe_tokens, tp_index * MOE_SHARE, MOE_SHARE, 0)
    own_normed = rms_rows(own_tokens, moe_gain)
    placed = dispatch_rows(own_normed[None], own_routes[None])[0]
    arrived = lax.all_to_all(placed, "ep", split_axis=0, concat_axis=1, tiled=True)
    hidden = expert_hidden(
        lax.all_gather(arrived[None], "tp", axis=0, tiled=True), gate_weight, up_weight
    )
    local_experts = hidden.shape[1]
    slot_count = hidden.shape[2]
    per_block = local_experts * slot_count
    partial_value = jnp.einsum(
        "besf,efd->besd", hidden, down_weight, preferred_element_type=jnp.float32
    )
    summed = lax.psum_scatter(
        partial_value.reshape(per_block * lax.axis_size("tp"), model_width),
        "tp",
        scatter_dimension=0,
        tiled=True,
    )
    results = summed.astype(jnp.bfloat16).reshape(
        local_experts, slot_count // CAP, CAP, model_width
    )
    returned = lax.all_to_all(results, "ep", split_axis=1, concat_axis=0, tiled=True).reshape(
        EXPERTS * CAP, model_width
    )
    weights = route_weights(own_normed, own_routes, router_group, router_expert)
    own_slots = own_routes * CAP + block_ranks(own_routes[None])[0]
    picked = jnp.take(returned, own_slots, axis=0).astype(jnp.float32)
    expert_out = jnp.sum(weights[:, :, None] * picked, axis=1).astype(jnp.bfloat16)
    return (mixer_out, expert_out)


def solution(mesh):
    return jax.shard_map(
        local,
        mesh=mesh,
        in_specs=(
            P("ep", None),
            P(),
            P(None, "tp"),
            P(None, "tp"),
            P(None, "tp"),
            P(None, "tp"),
            P("tp", None),
            P("ep", None),
            P(),
            P(),
            P(),
            P("ep", None),
            P("ep", None, "tp"),
            P("ep", None, "tp"),
            P("ep", "tp", None),
        ),
        out_specs=(P(("ep", "tp"), None), P(("ep", "tp"), None)),
        check_vma=False,
    )
```

profile of v0, /device:TPU:2, one launch (start us, length us, event | category | flops | bytes accessed | tf_op | source)
XLA Modules:
  0.0 281.7 jit_solution(8360812834643250856)
XLA Ops:
  7.2 0.0 all-gather.2.cloned.1.call-start
  7.2 0.8 constant_dynamic-slice_fusion
  8.1 0.1 copy.25
  8.1 0.1 eq.90
  8.2 0.1 fusion.48
  8.3 0.1 reduce_window_sum.12
  8.4 0.2 select_reduce_fusion
  8.6 0.1 squeeze_reshape.6
  8.6 0.1 copy.26
  8.7 0.8 compare_and_fusion
  9.5 0.1 convert_reduce_fusion
  9.6 1.0 fusion.37
  10.6 1.3 convolution_convert_fusion
  11.9 0.2 squeeze_reshape.7
  12.1 17.4 %all_to_all.8 = bf16[16,4,4096]{2,1,0:T(4,128)(2,1)S(1)} all-to-all(bf16[16,4,4096]{2,1,0:T(4,128)(2,1)S(1)} %squeeze_reshape.7), channel_id=1, replica_groups=mesh['ep'=16,'tp'=16] {'ep'}, dimensions={0} | all-to-all | bytes 1048576 | tf_op jit(solution)/shard_map/all_to_all | solution.py:120
  29.5 0.9 broadcast_in_dim.12
  30.5 0.0 all-gather.2.cloned.1.call-update
  30.5 0.0 reduce-scatter.5.cloned.1.call-start
  30.5 55.9 %all-gather.2.cloned.1.call-done = bf16[16,1,64,4096]{3,2,1,0:T(8,128)(2,1)} async-done(((bf16[1,1,64,4096]{3,2,1,0:T(8,128)(2,1)}), bf16[16,1,64,4096]{3,2,1,0:T(8,128)(2,1)}) %all-gather.2.cloned.1.call-update) | async-done | bytes 8388624 | tf_op jit(solution)/shard_map/all_gather | solution.py:122
  86.5 5.9 %fusion.7 = f32[16,1,64,128]{3,2,0,1:T(8,128)S(1)} fusion(bf16[16,1,64,4096]{3,2,1,0:T(8,128)(2,1)} %all-gather.2.cloned.1.call-done, bf16[1,4096,128]{2,1,0:T(8,128)(2,1)} %param.27), kind=kOutput, calls=%fused_computation.11 | convolution fusion | flops 1073741824 | bytes 9961472 | tf_op jit(solution)/shard_map/besd,edf->besf/dot_general | solution.py:63
  92.4 14.4 %fusion.23 = f32[16,64,4096]{2,1,0:T(8,128)} fusion(bf16[16,1,64,4096]{3,2,1,0:T(8,128)(2,1)} %all-gather.2.cloned.1.call-done, bf16[1,128,4096]{2,1,0:T(8,128)(2,1)S(1)} %copy-done, bf16[1,4096,128]{2,1,0:T(8,128)(2,1)S(1)} %copy-done.2, f32[16,1,64,128]{3,2,0,1:T(8,128)S(1)} %fusion.7), kind=kOutput, calls=%fused_computation.16 | convolution fusion | flops 2148270080 | bytes 27787264 | tf_op jit(solution)/shard_map/besf,efd->besd/dot_general | solution.py:127
  106.8 0.0 reduce-scatter.3.cloned.1.call-start
  106.9 1.5 copy-done.1
  108.4 0.5 fusion.4
  108.9 2.1 fusion.57
  111.0 0.9 fusion.26
  111.9 3.4 %collective-permute-start = (bf16[2,128]{1,0:T(2,128)(2,1)S(1)}, bf16[2,128]{1,0:T(2,128)(2,1)S(1)}, u32[]{:S(2)}, u32[]{:S(2)}) collective-permute-start(bf16[2,128]{1,0:T(2,128)(2,1)S(1)} %slice.34), channel_id=1, source_target_pairs={{0,16},{16,32},{32,48},{48,64},{64,80},{80,96},{96,112},{112,128},... | collective-permute-start | bytes 1544 | tf_op jit(solution)/shard_map/ppermute | solution.py:18
  115.3 2.1 collective-permute-done
  117.4 5.0 %fusion.27 = f32[256,4096]{1,0:T(8,128)} fusion(bf16[128,4096]{1,0:T(8,128)(2,1)} %param.21, bf16[4096,128]{1,0:T(8,128)(2,1)} %param.19, f32[258,128]{1,0:T(8,128)S(1)} %maximum_convert_fusion, f32[128]{0:T(128)S(1)} %get-tuple-element.7, f32[128]{0:T(128)S(1)} %get-tuple-element.8, f32[128]{0:T(128)S(1)} %get-tuple-element.6, ...), kind=kOutput, calls=%fused_computation.21 | convolution fusion | flops 541294592 | bytes 8800768 | tf_op jit(solution)/shard_map/dot_general | solution.py:86
  122.4 0.7 copy-done.4
  123.1 0.1 copy-done.8
  123.1 1.2 fusion.61
  124.3 1.1 fusion.53
  125.5 80.6 %reduce-scatter.5.cloned.1.call-done = f32[64,4096]{1,0:T(8,128)} async-done(((f32[1024,4096]{1,0:T(8,128)}), f32[64,4096]{1,0:T(8,128)}) %reduce-scatter.5.cloned.1.call-update) | async-done | bytes 1048592 | tf_op jit(solution)/shard_map/reduce_scatter | solution.py:130
  206.1 1.3 convert_element_type.92
  207.4 1.0 reshape.229
  208.4 7.3 %all-to-all-start.1 = ((bf16[1,16,4,4096]{3,2,0,1:T(4,128)(2,1)}), bf16[1,16,4,4096]{3,2,0,1:T(4,128)(2,1)S(1)}, u32[]{:S(2)}, u32[]{:S(2)}) async-start(bf16[1,16,4,4096]{3,2,0,1:T(4,128)(2,1)} %reshape.229), calls=%async_computation.3 | async-start | bytes 1048576 | tf_op jit(solution)/shard_map/all_to_all | solution.py:139
  215.6 0.2 select_reduce_fusion.1
  215.8 0.1 copy.28
  215.9 0.1 reshape.233
  216.0 0.1 copy.24
  216.1 0.1 copy.27
  216.2 54.8 %reduce-scatter.3.cloned.1.call-done = f32[16,4096]{1,0:T(8,128)} async-done(((f32[256,4096]{1,0:T(8,128)}), f32[16,4096]{1,0:T(8,128)}) %reduce-scatter.3.cloned.1.call-update) | async-done | bytes 262160 | tf_op jit(solution)/shard_map/reduce_scatter | solution.py:85
  271.0 1.6 convert_element_type.84
  272.7 0.1 reshape.230
  272.8 0.7 gather_fusion
  273.5 0.2 reshape.232
  273.7 1.5 multiply_reduce_fusion
  (29 shorter events, 0.2 us)
Async XLA Ops:
  7.2 85.2 %copy-start = (bf16[1,128,4096]{2,1,0:T(8,128)(2,1)S(1)}, bf16[1,128,4096]{2,1,0:T(8,128)(2,1)}, u32[]{:S(2)}) copy-start(bf16[1,128,4096]{2,1,0:T(8,128)(2,1)} %param.29) | copy-start | bytes 3145732
  7.2 79.3 %all-gather.2.cloned.1.call-start = ((), (), s32[]{:S(2)}) async-start(), calls=%async_computation.5 | async-start | bytes 8912896 | tf_op jit(solution)/shard_map/all_gather | solution.py:122
  30.5 61.9 %copy-start.2 = (bf16[1,4096,128]{2,1,0:T(8,128)(2,1)S(1)}, bf16[1,4096,128]{2,1,0:T(8,128)(2,1)}, u32[]{:S(2)}) copy-start(bf16[1,4096,128]{2,1,0:T(8,128)(2,1)} %param.28) | copy-start | bytes 3145732
  30.5 175.6 %reduce-scatter.5.cloned.1.call-start = ((), (), s32[]{:S(2)}) async-start(), calls=%async_computation.6 | async-start | bytes 17825792 | tf_op jit(solution)/shard_map/reduce_scatter | solution.py:130
  106.8 1.6 copy-start.1
  106.8 2.1 copy-start.3
  106.8 164.2 %reduce-scatter.3.cloned.1.call-start = ((), (), s32[]{:S(2)}) async-start(), calls=%async_computation.4 | async-start | bytes 4456448 | tf_op jit(solution)/shard_map/reduce_scatter | solution.py:85
  108.4 2.6 copy-start.6
  108.9 6.4 %copy-start.5 = (f32[3,128]{1,0:T(4,128)S(1)}, f32[3,128]{1,0:T(4,128)}, u32[]{:S(2)}) copy-start(f32[3,128]{1,0:T(4,128)} %param.20) | copy-start | bytes 4612
  111.9 5.5 %collective-permute-start = (bf16[2,128]{1,0:T(2,128)(2,1)S(1)}, bf16[2,128]{1,0:T(2,128)(2,1)S(1)}, u32[]{:S(2)}, u32[]{:S(2)}) collective-permute-start(bf16[2,128]{1,0:T(2,128)(2,1)S(1)} %slice.34), channel_id=1, source_target_pairs={{0,16},{16,32},{32,48},{48,64},{64,80},{80,96},{96,112},{112,128},... | collective-permute-start | bytes 1544 | tf_op jit(solution)/shard_map/ppermute | solution.py:18
  122.4 0.7 copy-start.4
  122.4 0.8 copy-start.8
  122.4 1.9 copy-start.7
  208.4 64.3 %all-to-all-start.1 = ((bf16[1,16,4,4096]{3,2,0,1:T(4,128)(2,1)}), bf16[1,16,4,4096]{3,2,0,1:T(4,128)(2,1)S(1)}, u32[]{:S(2)}, u32[]{:S(2)}) async-start(bf16[1,16,4,4096]{3,2,0,1:T(4,128)(2,1)} %reshape.229), calls=%async_computation.3 | async-start | bytes 1048576 | tf_op jit(solution)/shard_map/all_to_all | solution.py:139
Sparse Core Ops, SparseCore 0:
  30.6 55.8 all-gather.1
  107.0 99.0 reduce-scatter.4
  208.6 62.3 reduce-scatter.2
where the time goes:
time: 282 us
  waiting for transfers between devices  193 us (68%)
  matrix products  31.8 us (11%)
  blocking collectives  17.4 us (6%)
  between operations  14 us (5%)
  starting transfers between devices  10.8 us (4%)
  other arithmetic  7.33 us (3%)
  local copies, waits for them, and re-layouts  6.92 us (2%)
    reduce_scatter x1, waiting for transfers between devices, local(): lax.psum_scatter(partial_value.reshape(per_block * lax.axis_size('tp'), m...  80.6 us
    all_gather x1, waiting for transfers between devices, local(): lax.all_gather(arrived[None], 'tp', axis=0, tiled=True)  55.9 us
    reduce_scatter x1, waiting for transfers between devices, mixer_half(): lax.psum_scatter(jnp.dot(conv_out, mix_weight, preferred_element_type=jnp...  54.8 us
    all_to_all x1, blocking collectives, local(): lax.all_to_all(placed, 'ep', split_axis=0, concat_axis=1, tiled=True)  17.4 us
    dot_general x1, matrix products, local(): jnp.einsum('besf,efd->besd', hidden, down_weight, preferred_element_type=...  14.4 us
    all_to_all x1, starting transfers between devices, local(): lax.all_to_all(results, 'ep', split_axis=1, concat_axis=0, tiled=True)  7.27 us
    dot_general x1, matrix products, expert_hidden(): jnp.einsum('besd,edf->besf', arrived, gate_weight, preferred_element_type...  5.93 us
  transfers between devices with their start and end apart: 5, of which 4 were waited for; matrix products, arithmetic and copies ran while one was open for 5% of the time, Pallas kernels for 0%

commit v1 on v0

--- a/solution.py
+++ b/solution.py
@@ -10,6 +10,11 @@
 MOE_SHARE = 16
 EPG = 4
 CAP = 4
+
+
+def gather_from_all(x, axis, dim):
+    copies = jnp.concatenate([x] * lax.axis_size(axis), axis=dim)
+    return lax.all_to_all(copies, axis, dim, dim, tiled=True)
 
 
 def from_behind(value, axis, steps):
@@ -118,9 +123,7 @@
     own_normed = rms_rows(own_tokens, moe_gain)
     placed = dispatch_rows(own_normed[None], own_routes[None])[0]
     arrived = lax.all_to_all(placed, "ep", split_axis=0, concat_axis=1, tiled=True)
-    hidden = expert_hidden(
-        lax.all_gather(arrived[None], "tp", axis=0, tiled=True), gate_weight, up_weight
-    )
+    hidden = expert_hidden(gather_from_all(arrived[None], "tp", 0), gate_weight, up_weight)
     local_experts = hidden.shape[1]
     slot_count = hidden.shape[2]
     per_block = local_experts * slot_count

time: 282 us -> 417 us (1.48)
  blocking collectives: 17.4 us -> 210 us
  waiting for transfers between devices: 193 us -> 136 us
    all_to_all x0 -> x1, blocking collectives: none -> 193 us  [gather_from_all(): return lax.all_to_all(copies, axis, dim, dim, tiled=True)]
    all_gather x1 -> x0, waiting for transfers between devices: 55.9 us -> none  [local(): lax.all_gather(arrived[None], 'tp', axis=0, tiled=True)]
  transfers between devices with their start and end apart: 5 -> 4, of which waited for: 4 -> 3; matrix products, arithmetic and copies ran while one was open for 5% -> 4% of each run, Pallas kernels for 0% -> 0%
where the time goes in v1:
time: 417 us; the launch traced here: 416 us
  blocking collectives  210 us (50%)
  waiting for transfers between devices  136 us (33%)
  matrix products  28.1 us (7%)
  between operations  14.3 us (3%)
  local copies, waits for them, and re-layouts  10.4 us (2%)
  starting transfers between devices  9.45 us (2%)
  other arithmetic  7.33 us (2%)
    all_to_all x1, blocking collectives, gather_from_all(): return lax.all_to_all(copies, axis, dim, dim, tiled=True)  193 us
    reduce_scatter x1, waiting for transfers between devices, local(): lax.psum_scatter(partial_value.reshape(per_block * lax.axis_size('tp'), m...  77.8 us
    reduce_scatter x1, waiting for transfers between devices, mixer_half(): lax.psum_scatter(jnp.dot(conv_out, mix_weight, preferred_element_type=jnp...  54.8 us
    all_to_all x1, blocking collectives, local(): lax.all_to_all(placed, 'ep', split_axis=0, concat_axis=1, tiled=True)  17.4 us
    dot_general x1, matrix products, local(): jnp.einsum('besf,efd->besd', hidden, down_weight, preferred_element_type=...  14.4 us
  transfers between devices with their start and end apart: 4, of which 3 were waited for; matrix products, arithmetic and copies ran while one was open for 4% of the time, Pallas kernels for 0%

profile of v1, /device:TPU:2, one launch (start us, length us, event | category | flops | bytes accessed | tf_op | source)
XLA Modules:
  0.0 415.9 jit_solution(16299632416693376285)
XLA Ops:
  7.2 0.0 reduce-scatter.5.cloned.1.call-start
  7.2 0.8 constant_dynamic-slice_fusion
  8.1 0.1 copy.25
  8.1 0.1 eq.90
  8.2 0.1 fusion.48
  8.3 0.1 reduce_window_sum.12
  8.4 0.2 select_reduce_fusion
  8.6 0.1 squeeze_reshape.6
  8.6 0.1 copy.26
  8.7 0.8 compare_and_fusion
  9.5 0.1 convert_reduce_fusion
  9.6 1.0 fusion.37
  10.6 1.3 convolution_convert_fusion
  11.9 0.2 squeeze_reshape.7
  12.1 17.4 %all_to_all.23 = bf16[16,4,4096]{2,1,0:T(4,128)(2,1)S(1)} all-to-all(bf16[16,4,4096]{2,1,0:T(4,128)(2,1)S(1)} %squeeze_reshape.7), channel_id=1, replica_groups=mesh['ep'=16,'tp'=16] {'ep'}, dimensions={0} | all-to-all | bytes 1048576 | tf_op jit(solution)/shard_map/all_to_all | solution.py:125
  29.5 0.1 broadcast_in_dim.12
  29.7 1.0 concatenate.7
  30.7 193.0 %all_to_all.24 = bf16[16,1,64,4096]{3,2,1,0:T(8,128)(2,1)S(1)} all-to-all(bf16[16,1,64,4096]{3,2,1,0:T(8,128)(2,1)S(1)} %concatenate.7), channel_id=1, replica_groups=mesh['ep'=16,'tp'=16] {'tp'}, dimensions={0} | all-to-all | bytes 16777216 | tf_op jit(solution)/shard_map/all_to_all | solution.py:17
  223.7 3.2 copy-done.1
  226.9 2.3 fusion.7
  229.3 14.4 %fusion.23 = f32[16,64,4096]{2,1,0:T(8,128)} fusion(bf16[16,1,64,4096]{3,2,1,0:T(8,128)(2,1)} %copy-done.1, bf16[1,128,4096]{2,1,0:T(8,128)(2,1)S(1)} %copy-done, bf16[1,4096,128]{2,1,0:T(8,128)(2,1)S(1)} %copy-done.3, f32[16,1,64,128]{3,2,0,1:T(8,128)S(1)} %fusion.7), kind=kOutput, calls=%fused_computation.16 | convolution fusion | flops 2148270080 | bytes 27787264 | tf_op jit(solution)/shard_map/besf,efd->besd/dot_general | solution.py:130
  243.7 0.0 reduce-scatter.3.cloned.1.call-start
  243.7 1.5 copy-done.2
  245.2 0.5 fusion.4
  245.8 2.1 fusion.57
  247.8 0.9 fusion.26
  248.7 2.1 collective-permute-start
  250.9 3.3 collective-permute-done
  254.2 4.9 %fusion.27 = f32[256,4096]{1,0:T(8,128)} fusion(bf16[128,4096]{1,0:T(8,128)(2,1)} %param.21, bf16[4096,128]{1,0:T(8,128)(2,1)} %param.19, f32[258,128]{1,0:T(8,128)S(1)} %maximum_convert_fusion, f32[128]{0:T(128)S(1)} %get-tuple-element.7, f32[128]{0:T(128)S(1)} %get-tuple-element.8, f32[128]{0:T(128)S(1)} %get-tuple-element.6, ...), kind=kOutput, calls=%fused_computation.21 | convolution fusion | flops 541294592 | bytes 8800768 | tf_op jit(solution)/shard_map/dot_general | solution.py:91
  259.2 0.7 copy-done.5
  259.8 0.1 copy-done.10
  259.9 1.2 fusion.61
  261.1 1.1 fusion.53
  262.2 77.8 %reduce-scatter.5.cloned.1.call-done = f32[64,4096]{1,0:T(8,128)} async-done(((f32[1024,4096]{1,0:T(8,128)}), f32[64,4096]{1,0:T(8,128)}) %reduce-scatter.5.cloned.1.call-update) | async-done | bytes 1048592 | tf_op jit(solution)/shard_map/reduce_scatter | solution.py:133
  340.1 1.3 convert_element_type.92
  341.3 1.0 reshape.233
  342.3 7.3 %all-to-all-start.2 = ((bf16[1,16,4,4096]{3,2,0,1:T(4,128)(2,1)}), bf16[1,16,4,4096]{3,2,0,1:T(4,128)(2,1)S(1)}, u32[]{:S(2)}, u32[]{:S(2)}) async-start(bf16[1,16,4,4096]{3,2,0,1:T(4,128)(2,1)} %reshape.233), calls=%async_computation.4 | async-start | bytes 1048576 | tf_op jit(solution)/shard_map/all_to_all | solution.py:142
  349.6 0.2 select_reduce_fusion.1
  349.7 0.1 copy.28
  349.8 0.1 reshape.237
  350.0 0.1 copy.24
  350.0 0.1 copy.27
  350.2 54.8 %reduce-scatter.3.cloned.1.call-done = f32[16,4096]{1,0:T(8,128)} async-done(((f32[256,4096]{1,0:T(8,128)}), f32[16,4096]{1,0:T(8,128)}) %reduce-scatter.3.cloned.1.call-update) | async-done | bytes 262160 | tf_op jit(solution)/shard_map/reduce_scatter | solution.py:90
  405.0 1.6 convert_element_type.84
  406.6 0.1 reshape.234
  406.7 0.7 gather_fusion
  407.4 0.2 reshape.236
  407.6 1.5 multiply_reduce_fusion
  (32 shorter events, 0.2 us)
Async XLA Ops:
  7.2 222.1 %copy-start = (bf16[1,128,4096]{2,1,0:T(8,128)(2,1)S(1)}, bf16[1,128,4096]{2,1,0:T(8,128)(2,1)}, u32[]{:S(2)}) copy-start(bf16[1,128,4096]{2,1,0:T(8,128)(2,1)} %param.29) | copy-start | bytes 3145732
  7.2 332.9 %reduce-scatter.5.cloned.1.call-start = ((), (), s32[]{:S(2)}) async-start(), calls=%async_computation.6 | async-start | bytes 17825792 | tf_op jit(solution)/shard_map/reduce_scatter | solution.py:133
  30.7 196.2 %copy-start.7 = (bf16[1,4096,128]{2,1,0:T(8,128)(2,1)S(1)}, bf16[1,4096,128]{2,1,0:T(8,128)(2,1)}, u32[]{:S(2)}) copy-start(bf16[1,4096,128]{2,1,0:T(8,128)(2,1)} %param.27) | copy-start | bytes 3145732
  223.7 3.2 copy-start.1
  226.9 2.3 copy-start.3
  243.7 1.6 copy-start.2
  243.7 2.1 copy-start.4
  243.7 161.3 %reduce-scatter.3.cloned.1.call-start = ((), (), s32[]{:S(2)}) async-start(), calls=%async_computation.5 | async-start | bytes 4456448 | tf_op jit(solution)/shard_map/reduce_scatter | solution.py:90
  245.2 2.6 copy-start.8
  245.8 5.1 %copy-start.6 = (f32[3,128]{1,0:T(4,128)S(1)}, f32[3,128]{1,0:T(4,128)}, u32[]{:S(2)}) copy-start(f32[3,128]{1,0:T(4,128)} %param.20) | copy-start | bytes 4612
  248.7 5.5 %collective-permute-start = (bf16[2,128]{1,0:T(2,128)(2,1)S(1)}, bf16[2,128]{1,0:T(2,128)(2,1)S(1)}, u32[]{:S(2)}, u32[]{:S(2)}) collective-permute-start(bf16[2,128]{1,0:T(2,128)(2,1)S(1)} %slice.34), channel_id=1, source_target_pairs={{0,16},{16,32},{32,48},{48,64},{64,80},{80,96},{96,112},{112,128},... | collective-permute-start | bytes 1544 | tf_op jit(solution)/shard_map/ppermute | solution.py:23
  259.1 0.7 copy-start.5
  259.1 0.8 copy-start.10
  259.1 1.9 copy-start.9
  342.3 64.3 %all-to-all-start.2 = ((bf16[1,16,4,4096]{3,2,0,1:T(4,128)(2,1)}), bf16[1,16,4,4096]{3,2,0,1:T(4,128)(2,1)S(1)}, u32[]{:S(2)}, u32[]{:S(2)}) async-start(bf16[1,16,4,4096]{3,2,0,1:T(4,128)(2,1)} %reshape.233), calls=%async_computation.4 | async-start | bytes 1048576 | tf_op jit(solution)/shard_map/all_to_all | solution.py:142
Sparse Core Ops, SparseCore 0:
  243.8 96.2 reduce-scatter.4
  342.6 62.3 reduce-scatter.2
